TPU v7x, 32 devices: a whole 2x2x4 slice. The times are simulated.
32 devices in a mesh: sp: 8 (over z, y), tp: 4 (over x, core).
Axes of the slice: x: 2, y: 2, z: 4, core: 2. Of those that a mesh axis runs over, the one named last changes fastest.
Arguments:
- tokens: bfloat16 [2048, 4096], P(('sp', 'tp')), may hold values from -700 to 700
- down_query: bfloat16 [4096, 1024], replicated, may hold values from -0.09375 to 0.09375
- down_latent: bfloat16 [4096, 512], replicated, may hold values from -0.09375 to 0.09375
- down_rotary: bfloat16 [4096, 64], replicated, may hold values from -0.09375 to 0.09375
- query_gain: float32 [1024], replicated, may hold values from 0.1 to 1.9
- latent_gain: float32 [512], replicated, may hold values from 0.1 to 1.9
- up_query: bfloat16 [1024, 2048], P(None, 'tp'), may hold values from -0.1875 to 0.1875
- up_query_rotary: bfloat16 [1024, 1024], P(None, 'tp'), may hold values from -0.1875 to 0.1875
- up_key: bfloat16 [512, 2048], P(None, 'tp'), may hold values from -0.25 to 0.25
- up_value: bfloat16 [512, 2048], P(None, 'tp'), may hold values from -0.25 to 0.25
- out_weight: bfloat16 [2048, 4096], P('tp'), may hold values from -0.39648438 to 0.39648438
Outputs:
- mixed: bfloat16 [2048, 4096], P(('sp', 'tp'))
All inputs are finite; a program needn't handle non-finite values.
Results may differ from a plain program's by a relative error of at most 0.03.
Values may be sent and summed in bfloat16 or wider, within the bound.
A program may use at most 192 MiB of HBM per device.

v0:
```python
import jax
import jax.numpy as jnp
from jax import lax
from jax.sharding import PartitionSpec as P

NOPE = 128
ROPE = 64
VDIM = 128


rope_base = 500000.0
norm_eps = 1e-06
masked_score = -1e30


def rotate_half(values, positions):
    half = values.shape[-1] // 2
    inverse = rope_base ** (-jnp.arange(0, 2 * half, 2, dtype=jnp.float32) / (2 * half))
    angles = positions.astype(jnp.float32)[:, None] * inverse
    if values.ndim == 3:
        angles = angles[:, None, :]
    cosine = jnp.cos(angles)
    sine = jnp.sin(angles)
    first = values[..., :half]
    second = values[..., half:]
    return jnp.concatenate(
        [first * cosine - second * sine, second * cosine + first * sine], axis=-1
    )


def norm_rows(values, gain):
    return values * lax.rsqrt(jnp.mean(values * values, axis=-1, keepdims=True) + norm_eps) * gain


def local(
    tokens,
    down_query,
    down_latent,
    down_rotary,
    query_gain,
    latent_gain,
    up_query,
    up_query_rotary,
    up_key,
    up_value,
    out_weight,
):
    own_count = tokens.shape[0]
    seq_index = lax.axis_index("sp")
    own_start = (seq_index * lax.axis_size("tp") + lax.axis_index("tp")) * own_count
    own_positions = own_start + jnp.arange(own_count, dtype=jnp.int32)
    query_latent = norm_rows(
        jnp.dot(tokens, down_query, preferred_element_type=jnp.float32), query_gain
    ).astype(jnp.bfloat16)
    kv_latent = norm_rows(
        jnp.dot(tokens, down_latent, preferred_element_type=jnp.float32), latent_gain
    ).astype(jnp.bfloat16)
    key_rotary = rotate_half(
        jnp.dot(tokens, down_rotary, preferred_element_type=jnp.float32), own_positions
    ).astype(jnp.bfloat16)
    query_rows, latent_rows, rotary_rows = (
        lax.all_gather(query_latent, "tp", axis=0, tiled=True),
        lax.all_gather(kv_latent, "tp", axis=0, tiled=True),
        lax.all_gather(key_rotary, "tp", axis=0, tiled=True),
    )
    span = query_rows.shape[0]
    heads = up_key.shape[1] // NOPE
    query_positions = seq_index * span + jnp.arange(span, dtype=jnp.int32)
    last_position = seq_index * span + span - 1
    query_plain = (
        jnp.dot(query_rows, up_query, preferred_element_type=jnp.float32)
        .astype(jnp.bfloat16)
        .reshape(span, heads, NOPE)
    )
    query_turned = rotate_half(
        jnp.dot(query_rows, up_query_rotary, preferred_element_type=jnp.float32).reshape(
            span, heads, ROPE
        ),
        query_positions,
    ).astype(jnp.bfloat16)
    factor = (NOPE + ROPE) ** (-0.5)
    start_state = (
        jnp.full((heads, span), masked_score, jnp.float32),
        jnp.zeros((heads, span), jnp.float32),
        jnp.zeros((span, heads, VDIM), jnp.float32),
    )
    pieces = (
        lax.all_gather(latent_rows, "sp", axis=0, tiled=True),
        lax.all_gather(rotary_rows, "sp", axis=0, tiled=True),
    )

    def make_keys():
        latent_piece, turned_piece = pieces
        key_count = latent_piece.shape[0]
        key_plain = (
            jnp.dot(latent_piece, up_key, preferred_element_type=jnp.float32)
            .astype(jnp.bfloat16)
            .reshape(key_count, heads, NOPE)
        )
        key_values = (
            jnp.dot(latent_piece, up_value, preferred_element_type=jnp.float32)
            .astype(jnp.bfloat16)
            .reshape(key_count, heads, VDIM)
        )
        return (key_plain, key_values, turned_piece)

    def update(state):
        best, total, summed = state
        key_plain, key_values, key_turned = make_keys()
        key_count = key_plain.shape[0]
        key_positions = jnp.arange(key_count, dtype=jnp.int32)
        scores = jnp.einsum(
            "qhd,khd->hqk", query_plain, key_plain, preferred_element_type=jnp.float32
        )
        scores = scores + jnp.einsum(
            "qhr,kr->hqk", query_turned, key_turned, preferred_element_type=jnp.float32
        )
        scores = scores * factor
        allowed = (key_positions[None, :] <= query_positions[:, None])[None]
        scores = jnp.where(allowed, scores, masked_score)
        new_best = jnp.maximum(best, jnp.max(scores, axis=-1))
        weights = jnp.where(allowed, jnp.exp(scores - new_best[..., None]), 0.0)
        total = jnp.sum(weights, axis=-1)
        added = jnp.einsum(
            "hqk,khd->qhd",
            weights.astype(jnp.bfloat16),
            key_values,
            preferred_element_type=jnp.float32,
        )
        summed = added
        return (new_best, total, summed)

    def keep(state):
        return state

    best, total, summed = lax.cond(jnp.int32(0) <= last_position, update, keep, start_state)
    attended = (
        (summed / jnp.transpose(total)[:, :, None]).astype(jnp.bfloat16).reshape(span, heads * VDIM)
    )
    return lax.psum_scatter(
        jnp.dot(attended, out_weight, preferred_element_type=jnp.float32).astype(jnp.bfloat16),
        "tp",
        scatter_dimension=0,
        tiled=True,
    )


def solution(mesh):
    return jax.shard_map(
        local,
        mesh=mesh,
        in_specs=(
            P(("sp", "tp"), None),
            P(),
            P(),
            P(),
            P(),
            P(),
            P(None, "tp"),
            P(None, "tp"),
            P(None, "tp"),
            P(None, "tp"),
            P("tp", None),
        ),
        out_specs=P(("sp", "tp"), None),
        check_vma=False,
    )
```

profile of v0, /device:TPU:28, one launch (start us, length us, event | category | flops | bytes accessed | tf_op | source)
XLA Modules:
  0.0 123.0 jit_solution(8975312831626569920)
XLA Ops:
  6.5 0.0 copy-start
  6.5 0.0 copy-start.1
  6.5 0.0 copy-start.5
  6.5 0.0 copy-start.2
  6.5 0.0 all-gather.2.cloned.1.call-start
  6.6 3.4 %multiply_reduce_fusion.1 = (f32[64]{0:T(128)S(1)}, f32[64,512]{1,0:T(8,128)S(1)}) fusion(bf16[64,4096]{1,0:T(8,128)(2,1)} %param.13, bf16[4096,512]{1,0:T(8,128)(2,1)} %param.15), kind=kOutput, calls=%fused_computation.30 | convolution fusion | flops 268500928 | bytes 4849920 | tf_op jit(solution)/shard_map/dot_general | solution.py:56
  10.0 0.0 copy-done.5
  10.0 0.1 multiply_convert_fusion.1
  10.1 6.2 %all_gather.15 = bf16[256,512]{1,0:T(8,128)(2,1)} all-gather(bf16[64,512]{1,0:T(8,128)(2,1)S(1)} %multiply_convert_fusion.1), channel_id=1, replica_groups=mesh['sp'=8,'tp'=4] {'tp'}, dimensions={0}, use_global_device_ids=true | all-gather | bytes 327680 | tf_op jit(solution)/shard_map/all_gather | solution.py:63
  16.4 0.0 all-gather.2.cloned.1.call-update
  16.4 0.0 reduce-scatter.2.cloned.1.call-start
  16.5 0.0 copy-done.1
  16.5 0.0 copy-done.2
  16.5 0.3 fusion.26
  16.8 0.1 fusion.22
  16.9 0.1 copy.20
  17.0 5.2 %all_gather.18 = bf16[256,64]{1,0:T(8,128)(2,1)S(1)} all-gather(bf16[64,64]{1,0:T(8,128)(2,1)S(1)} %copy.20), channel_id=1, replica_groups=mesh['sp'=8,'tp'=4] {'tp'}, dimensions={0}, use_global_device_ids=true | all-gather | bytes 40960 | tf_op jit(solution)/shard_map/all_gather | solution.py:64
  22.3 32.7 %all_gather.19 = bf16[2048,64]{1,0:T(8,128)(2,1)S(1)} all-gather(bf16[256,64]{1,0:T(8,128)(2,1)S(1)} %all_gather.18), channel_id=1, replica_groups=mesh['sp'=8,'tp'=4] {'sp'}, dimensions={0}, use_global_device_ids=true | all-gather | bytes 294912 | tf_op jit(solution)/shard_map/all_gather | solution.py:89
  55.0 0.0 copy-start.4
  55.0 0.0 copy-start.3
  55.0 5.1 %multiply_reduce_fusion = (f32[64]{0:T(128)S(1)}, f32[64,1024]{1,0:T(8,128)S(1)}) fusion(bf16[64,4096]{1,0:T(8,128)(2,1)S(1)} %copy-done.1, bf16[4096,1024]{1,0:T(8,128)(2,1)} %param.14), kind=kOutput, calls=%fused_computation.25 | convolution fusion | flops 537001920 | bytes 9175296 | tf_op jit(solution)/shard_map/dot_general | solution.py:53
  60.1 0.0 copy-start.7
  60.1 0.0 copy-start.8
  60.1 0.0 copy-done.4
  60.1 0.1 multiply_convert_fusion
  60.2 7.4 %all_gather.17 = bf16[256,1024]{1,0:T(8,128)(2,1)S(1)} all-gather(bf16[64,1024]{1,0:T(8,128)(2,1)S(1)} %multiply_convert_fusion), channel_id=1, replica_groups=mesh['sp'=8,'tp'=4] {'tp'}, dimensions={0}, use_global_device_ids=true | all-gather | bytes 655360 | tf_op jit(solution)/shard_map/all_gather | solution.py:62
  67.6 0.2 multiply_cosine_fusion
  67.8 0.0 copy-done.3
  67.8 0.4 fusion.27
  68.2 0.0 copy-done
  68.3 0.4 convolution_convert_fusion.3
  68.7 0.0 all-gather.2.cloned.1.call-done
  68.7 0.0 copy-done.7
  68.7 0.0 copy-done.8
  68.8 10.9 %conditional.1 = (f32[4,256]{1,0:T(4,128)S(1)}, f32[256,4,128]{0,2,1:T(8,128)S(1)}) conditional(s32[]{:T(128)} %convert_element_type.43, () %tuple.13, (s32[]{:T(128)}, s32[256]{0:T(256)S(1)}, bf16[2048,512]{1,0:T(8,128)(2,1)}, bf16[512,512]{1,0:T(8,128)(2,1)S(1)}, bf16[256,512]{1,0:T(8,128)(2,1)S(1)}, /*index=5*/bf16[2048,64]{1,0:T(8,128)(2,1)S(1)}, ...), branch_computations={%region_2.0_spmd, %region_3.6_spmd} | conditional | flops 3513253120 | bytes 67267632 | solution.py:136
  68.8 0.3 iota_compare_fusion
  69.1 2.9 %convolution_convert_fusion.1 = bf16[2048,512]{0,1:T(8,128)(2,1)S(1)} fusion(bf16[2048,512]{1,0:T(8,128)(2,1)} %get-tuple-element.26, bf16[512,512]{1,0:T(8,128)(2,1)S(1)} %get-tuple-element.38), kind=kOutput, calls=%fused_computation.11 | convolution fusion | flops 1074790400 | bytes 4718592 | tf_op jit(solution)/shard_map/cond/branch_1_fun/dot_general | solution.py:96
  72.0 1.3 %fusion.13 = f32[4,2048,256]{2,1,0:T(8,128)S(1)} fusion(bf16[2048,4,128]{0,2,1:T(8,128)(2,1)S(1)} %bitcast.46, bf16[256,512]{1,0:T(8,128)(2,1)S(1)} %get-tuple-element.28), kind=kOutput, calls=%fused_computation.15 | convolution fusion | flops 536870912 | bytes 10747904 | tf_op jit(solution)/shard_map/cond/branch_1_fun/qhd,khd->hqk/dot_general | solution.py:112
  73.3 0.0 copy-start.6
  73.3 1.8 %fusion.25 = (f32[4,256]{1,0:T(4,128)S(1)}, f32[4,256,2048]{1,2,0:T(8,128)S(1)}) fusion(bf16[256,4,64]{0,2,1:T(8,128)(2,1)S(1)} %get-tuple-element.30, bf16[2048,64]{1,0:T(8,128)(2,1)S(1)} %get-tuple-element.45, f32[4,2048,256]{2,1,0:T(8,128)S(1)} %fusion.13, pred[256,2048]{0,1:T(8,128)(4,1)S(1)} %iota_compare_fusion), kind=kOutput, calls=%fused_computation.49 | convolution fusion | flops 276823040 | bytes 17698816 | tf_op jit(solution)/shard_map/cond/branch_1_fun/qhr,kr->hqk/dot_general | solution.py:115
  75.2 0.0 copy-done.6
  75.2 1.3 %convolution_convert_fusion = bf16[2048,512]{0,1:T(8,128)(2,1)S(1)} fusion(bf16[2048,512]{1,0:T(8,128)(2,1)S(1)} %copy-done.6, bf16[512,512]{1,0:T(8,128)(2,1)S(1)} %get-tuple-element.39), kind=kOutput, calls=%fused_computation.10 | convolution fusion | flops 1074790400 | bytes 4718592 | tf_op jit(solution)/shard_map/cond/branch_1_fun/dot_general | solution.py:101
  76.5 1.7 %fusion.9 = f32[256,4,128]{0,2,1:T(8,128)S(1)} fusion(bf16[2048,4,128]{0,2,1:T(8,128)(2,1)S(1)} %bitcast.50, f32[4,256,2048]{1,2,0:T(8,128)S(1)} %get-tuple-element.49, f32[4,256]{1,0:T(4,128)S(1)} %broadcast_maximum_fusion, pred[256,2048]{0,1:T(8,128)(4,1)S(1)} %iota_compare_fusion), kind=kOutput, calls=%fused_computation.13 | convolution fusion | flops 543162368 | bytes 11538432 | tf_op jit(solution)/shard_map/cond/branch_1_fun/hqk,khd->qhd/dot_general | solution.py:124
  78.2 1.5 %fusion.3 = f32[4,256]{1,0:T(4,128)S(1)} fusion(f32[4,256,2048]{1,2,0:T(8,128)S(1)} %get-tuple-element.49, f32[4,256]{1,0:T(4,128)S(1)} %broadcast_maximum_fusion, pred[256,2048]{0,1:T(8,128)(4,1)S(1)} %iota_compare_fusion), kind=kLoop, calls=%fused_computation.5 | loop fusion | flops 6290432 | bytes 8921088 | tf_op jit(solution)/shard_map/cond/branch_1_fun/reduce_sum | solution.py:123
  79.8 4.8 %convolution_convert_fusion.2 = bf16[256,4096]{1,0:T(8,128)(2,1)} fusion(bf16[256,512]{0,1:T(8,128)(2,1)S(1)} %bitcast.47, bf16[512,4096]{1,0:T(8,128)(2,1)} %param.23), kind=kOutput, calls=%fused_computation.21 | convolution fusion | flops 1074790400 | bytes 6553600 | tf_op jit(solution)/shard_map/dot_general | solution.py:141
  84.6 0.0 reduce-scatter.2.cloned.1.call-update
  84.6 31.6 %reduce-scatter.2.cloned.1.call-done = bf16[64,4096]{1,0:T(8,128)(2,1)} async-done(((bf16[256,4096]{1,0:T(8,128)(2,1)}), bf16[64,4096]{1,0:T(8,128)(2,1)}) %reduce-scatter.2.cloned.1.call-update) | async-done | bytes 524304 | tf_op jit(solution)/shard_map/reduce_scatter | solution.py:140
  (12 shorter events, 0.1 us)
Async XLA Ops:
  6.5 61.7 %copy-start = (bf16[1024,512]{1,0:T(8,128)(2,1)S(1)}, bf16[1024,512]{1,0:T(8,128)(2,1)}, u32[]{:S(2)}) copy-start(bf16[1024,512]{1,0:T(8,128)(2,1)} %param.19) | copy-start | bytes 3145732
  6.5 9.9 %copy-start.1 = (bf16[64,4096]{1,0:T(8,128)(2,1)S(1)}, bf16[64,4096]{1,0:T(8,128)(2,1)}, u32[]{:S(2)}) copy-start(bf16[64,4096]{1,0:T(8,128)(2,1)} %param.13) | copy-start | bytes 1572868
  6.5 3.5 %copy-start.5 = (f32[512]{0:T(512)S(1)}, f32[512]{0:T(512)}, u32[]{:S(2)}) copy-start(f32[512]{0:T(512)} %param.18) | copy-start | bytes 6148
  6.5 9.9 %copy-start.2 = (bf16[4096,64]{0,1:T(8,128)(2,1)S(1)}, bf16[4096,64]{0,1:T(8,128)(2,1)}, u32[]{:S(2)}) copy-start(bf16[4096,64]{0,1:T(8,128)(2,1)} %param.16) | copy-start | bytes 1572868
  6.5 62.2 %all-gather.2.cloned.1.call-start = ((), (), s32[]{:S(2)}) async-start(), calls=%async_computation.1 | async-start | bytes 2359296 | tf_op jit(solution)/shard_map/all_gather | solution.py:88
  16.4 99.8 %reduce-scatter.2.cloned.1.call-start = ((), (), s32[]{:S(2)}) async-start(), calls=%async_computation.2 | async-start | bytes 2621440 | tf_op jit(solution)/shard_map/reduce_scatter | solution.py:140
  55.0 5.2 %copy-start.4 = (f32[1024]{0:T(1024)S(1)}, f32[1024]{0:T(1024)}, u32[]{:S(2)}) copy-start(f32[1024]{0:T(1024)} %param.17) | copy-start | bytes 12292
  55.0 12.9 %copy-start.3 = (bf16[1024,256]{1,0:T(8,128)(2,1)S(1)}, bf16[1024,256]{1,0:T(8,128)(2,1)}, u32[]{:S(2)}) copy-start(bf16[1024,256]{1,0:T(8,128)(2,1)} %param.20) | copy-start | bytes 1572868
  60.1 8.7 %copy-start.7 = (bf16[512,512]{1,0:T(8,128)(2,1)S(1)}, bf16[512,512]{1,0:T(8,128)(2,1)}, u32[]{:S(2)}) copy-start(bf16[512,512]{1,0:T(8,128)(2,1)} %param.21) | copy-start | bytes 1572868
  60.1 8.6 %copy-start.8 = (bf16[512,512]{1,0:T(8,128)(2,1)S(1)}, bf16[512,512]{1,0:T(8,128)(2,1)}, u32[]{:S(2)}) copy-start(bf16[512,512]{1,0:T(8,128)(2,1)} %param.22) | copy-start | bytes 1572868
  73.3 1.8 %copy-start.6 = (bf16[2048,512]{1,0:T(8,128)(2,1)S(1)}, bf16[2048,512]{1,0:T(8,128)(2,1)}, u32[]{:S(2)}) copy-start(bf16[2048,512]{1,0:T(8,128)(2,1)} %get-tuple-element.26) | copy-start | bytes 6291460 | tf_op jit(solution)/shard_map/cond
Sparse Core Ops, SparseCore 0:
  16.5 50.1 all-gather.1
  84.7 31.4 reduce-scatter.1
where the time goes:
time: 125 us; the launch traced here: 123 us
  blocking collectives  51.5 us (41%)
  waiting for transfers between devices  31.6 us (25%)
  matrix products  23.4 us (19%)
  between operations  13.6 us (11%)
  other arithmetic  2.51 us (2%)
    all_gather x1, blocking collectives, local(): lax.all_gather(rotary_rows, 'sp', axis=0, tiled=True)  32.7 us
    reduce_scatter x1, waiting for transfers between devices, local(): lax.psum_scatter(jnp.dot(attended, out_weight, preferred_element_type=jnp...  31.6 us
    all_gather x1, blocking collectives, local(): lax.all_gather(query_latent, 'tp', axis=0, tiled=True)  7.38 us
    all_gather x1, blocking collectives, local(): lax.all_gather(kv_latent, 'tp', axis=0, tiled=True)  6.23 us
    all_gather x1, blocking collectives, local(): lax.all_gather(key_rotary, 'tp', axis=0, tiled=True)  5.24 us
    dot_general x1, matrix products, local(): jnp.dot(tokens, down_query, preferred_element_type=jnp.float32)  5.12 us
    dot_general x1, matrix products, local(): jnp.dot(attended, out_weight, preferred_element_type=jnp.float32)  4.81 us
    dot_general x1, matrix products, local(): jnp.dot(tokens, down_latent, preferred_element_type=jnp.float32)  3.43 us
  transfers between devices with their start and end apart: 2, of which 1 were waited for; matrix products, arithmetic and copies ran while one was open for 6% of the time, Pallas kernels for 0%

commit v1 on v0

v1 whole, which is shorter than its diff:
```python
import functools

import jax
import jax.numpy as jnp
from jax import lax
from jax.experimental import pallas as pl
from jax.experimental.pallas import tpu as pltpu
from jax.sharding import PartitionSpec as P

NOPE = 128
ROPE = 64
VDIM = 128
LANES = 128

rope_base = 500000.0
norm_eps = 1e-06
masked_score = -1e30
log2e = 1.4426950408889634

MESH = pl.DeviceIdType.MESH
F32 = jnp.float32
BF16 = jnp.bfloat16


def dot(a, b):
    return jnp.dot(a, b, preferred_element_type=F32)


def turn(v, cosine, sine):
    lane = lax.broadcasted_iota(jnp.int32, v.shape, 1)
    other = jnp.where(lane % ROPE < ROPE // 2, pltpu.roll(v, LANES - ROPE // 2, 1), pltpu.roll(v, ROPE // 2, 1))
    return v * cosine + other * sine


def normed(v, gain):
    return v * lax.rsqrt(jnp.mean(v * v, axis=-1, keepdims=True) + norm_eps) * gain


def kernel(
    S,
    T,
    chunks,
    pieces,
    tokens_hbm,
    dq_hbm,
    dl_hbm,
    dr_hbm,
    qg_ref,
    lg_ref,
    uq_hbm,
    ur_hbm,
    uk_hbm,
    uv_hbm,
    ow_hbm,
    cos_ref,
    sin_ref,
    out_ref,
    tokens,
    dq,
    dl,
    dr,
    uq,
    ur,
    uk,
    uv,
    ow,
    kv,
    ql,
    qh,
    acc,
    best,
    att,
    pair_out,
    pair_in,
    kept,
    cross_out,
    cross_in,
    load_sem,
    kv_send,
    kv_recv,
    q_send,
    q_recv,
    pair_send,
    pair_recv,
    cross_send,
    cross_recv,
):
    O = S // 2
    rows = tokens.shape[0]
    span = rows * T
    depth = tokens.shape[1]
    heads = qh.shape[0]
    rank = dl.shape[1]
    sp = lax.axis_index("sp")
    tp = lax.axis_index("tp")
    o, i = sp // 2, sp % 2
    g, c = tp // 2, tp % 2

    def dev(o_, i_, g_, c_):
        return {"sp": o_ * 2 + i_, "tp": g_ * 2 + c_}

    across = dev(o, i, 1 - g, c)
    beside = dev(o, 1 - i, g, c)
    mate = dev(o, i, g, 1 - c)

    step = depth // chunks
    loads = []

    def load(src, dst):
        copy = pltpu.make_async_copy(src, dst, load_sem.at[len(loads)])
        loads.append(copy)
        copy.start()
        return copy

    tok_load = load(tokens_hbm, tokens)
    dl_loads = [load(dl_hbm.at[pl.ds(k * step, step)], dl.at[pl.ds(k * step, step)]) for k in range(chunks)]
    dr_load = load(dr_hbm, dr)
    dq_loads = [load(dq_hbm.at[pl.ds(k * step, step)], dq.at[pl.ds(k * step, step)]) for k in range(chunks)]
    up_loads = [load(uq_hbm, uq), load(ur_hbm, ur), load(uk_hbm, uk), load(uv_hbm, uv)]
    ow_load = load(ow_hbm, ow)

    barrier = pltpu.get_barrier_semaphore()
    for d in range(1, O):
        pl.semaphore_signal(barrier, inc=1, device_id=dev((o + d) % O, i, g, c), device_id_type=MESH)
    for target in (across, beside, mate):
        pl.semaphore_signal(barrier, inc=1, device_id=target, device_id_type=MESH)

    def block(o_, i_, g_, c_):
        return (o_ * 2 + i_) * T + g_ * 2 + c_

    def block_rows(b):
        return pl.ds(pl.multiple_of(b * rows, rows), rows)

    def kv_copy(b, target, index):
        part = kv.at[block_rows(b)]
        return pltpu.make_async_remote_copy(
            src_ref=part,
            dst_ref=part,
            send_sem=kv_send.at[index],
            recv_sem=kv_recv.at[b],
            device_id=target,
            device_id_type=MESH,
        )

    def kv_wait(b):
        kv_copy(b, mate, 0).wait_recv()

    tok_load.wait()
    latent = jnp.zeros((rows, rank), F32)
    for k in range(chunks):
        dl_loads[k].wait()
        latent += dot(tokens[:, k * step : (k + 1) * step], dl[k * step : (k + 1) * step, :])
    dr_load.wait()
    turned = dot(tokens[...], dr[...])
    turned = jnp.concatenate([turned, jnp.zeros((rows, LANES - ROPE), F32)], axis=1)
    own_rows = pl.ds(pl.multiple_of(tp * rows, rows), rows)
    mine = block_rows(block(o, i, g, c))
    kv[mine, :rank] = normed(latent, lg_ref[...]).astype(BF16)
    kv[mine, rank:] = turn(turned, cos_ref[own_rows, :], sin_ref[own_rows, :]).astype(BF16)

    pl.semaphore_wait(barrier, O - 1 + 3)

    def up_copy(d):
        return kv_copy(block(o, i, g, c), dev((o + d) % O, i, g, c), d)

    def relay_near(d, act):
        b = block(o - d, i, g, c)
        act(kv_copy(b, across, O + d))

        @pl.when((i == 0) | (d > 0))
        def _():
            act(kv_copy(b, beside, 2 * O + 2 * d))

        act(kv_copy(b, mate, 4 * O + 4 * d))

    def relay_far(d, act):
        b = block(o - d, i, 1 - g, c)

        @pl.when((i == 0) | (d > 0))
        def _():
            act(kv_copy(b, beside, 2 * O + 2 * d + 1))

        act(kv_copy(b, mate, 4 * O + 4 * d + 1))

    def relay_beside(d, act):
        act(kv_copy(block(o - d, 1 - i, g, c), mate, 4 * O + 4 * d + 2))
        act(kv_copy(block(o - d, 1 - i, 1 - g, c), mate, 4 * O + 4 * d + 3))

    def start(copy):
        copy.start()

    def sent(copy):
        copy.wait_send()

    def relay(d):
        kv_wait(block(o - d, i, g, c))
        relay_near(d, start)
        kv_wait(block(o - d, i, 1 - g, c))
        relay_far(d, start)

    for d in range(1, O):

        @pl.when(o + d < O)
        def _(d=d):
            up_copy(d).start()

    relay_near(0, start)

    query = jnp.zeros((rows, dq.shape[1]), F32)
    for k in range(chunks):
        dq_loads[k].wait()
        query += dot(tokens[:, k * step : (k + 1) * step], dq[k * step : (k + 1) * step, :])
        if k == chunks // 2 - 1:
            kv_wait(block(o, i, 1 - g, c))
            relay_far(0, start)
    ql[own_rows, :] = normed(query, qg_ref[...]).astype(BF16)

    def q_copy(t, target, index):
        part = ql.at[block_rows(t)]
        return pltpu.make_async_remote_copy(
            src_ref=part,
            dst_ref=part,
            send_sem=q_send.at[index],
            recv_sem=q_recv.at[t],
            device_id=target,
            device_id_type=MESH,
        )

    far = (1 - g) * 2 + c
    q_copies = [q_copy(tp, across, 0), q_copy(tp, mate, 1), q_copy(far, mate, 2)]
    q_copies[0].start()
    q_copies[1].start()

    @pl.when(o >= 1)
    def _():
        relay(1)

    q_copy(far, mate, 2).wait_recv()
    q_copies[2].start()
    q_copy(g * 2 + 1 - c, mate, 0).wait_recv()
    q_copy((1 - g) * 2 + 1 - c, mate, 0).wait_recv()

    for copy in up_loads:
        copy.wait()
    plain = dot(ql[...], uq[...]).astype(BF16)
    turning = dot(ql[...], ur[...])
    low = lax.broadcasted_iota(jnp.int32, (span, LANES), 1) < ROPE
    for pair in range(heads // 2):
        both = turn(turning[:, pair * LANES : (pair + 1) * LANES], cos_ref[...], sin_ref[...])
        qh[2 * pair, :, NOPE:] = jnp.where(low, both, 0.0).astype(BF16)
        qh[2 * pair + 1, :, NOPE:] = jnp.where(low, pltpu.roll(both, ROPE, 1), 0.0).astype(BF16)
    for h in range(heads):
        qh[h, :, :NOPE] = plain[:, h * NOPE : (h + 1) * NOPE]
        best[h] = jnp.full((span, LANES), masked_score, F32)
        acc[h] = jnp.zeros((span, 2 * VDIM), F32)

    scale = (NOPE + ROPE) ** (-0.5) * log2e

    def attend(s):
        part = pl.ds(pl.multiple_of(s * span, span), span)
        lat = kv[part, :rank]
        rot = kv[part, rank:]
        keys = dot(lat, uk[...]).astype(BF16)
        values = dot(lat, uv[...]).astype(BF16)
        ones = jnp.ones((span, VDIM), BF16)
        q_pos = sp * span + lax.broadcasted_iota(jnp.int32, (span, span), 0)
        k_pos = s * span + lax.broadcasted_iota(jnp.int32, (span, span), 1)
        allowed = k_pos <= q_pos
        for h in range(heads):
            key = jnp.concatenate([keys[:, h * NOPE : (h + 1) * NOPE], rot], axis=1)
            value = jnp.concatenate([values[:, h * VDIM : (h + 1) * VDIM], ones], axis=1)
            scores = lax.dot_general(qh[h], key, (((1,), (1,)), ((), ())), preferred_element_type=F32)
            scores = jnp.where(allowed, scores * scale, masked_score)
            old = best[h][:, :1]
            new = jnp.maximum(old, jnp.max(scores, axis=-1, keepdims=True))
            weights = jnp.exp2(scores - new).astype(BF16)
            acc[h] = acc[h] * jnp.exp2(old - new) + dot(weights, value)
            best[h] = jnp.broadcast_to(new, (span, LANES))

    def visit(d, carry):
        @pl.when(d + 2 <= o)
        def _():
            relay(d + 2)

        kv_wait(block(o - d, i, g, 1 - c))
        kv_wait(block(o - d, i, 1 - g, 1 - c))
        attend((o - d) * 2 + i)

        @pl.when((i == 1) | (d > 0))
        def _():
            kv_wait(block(o - d, 1 - i, g, c))
            kv_wait(block(o - d, 1 - i, 1 - g, c))
            relay_beside(d, start)
            kv_wait(block(o - d, 1 - i, g, 1 - c))
            kv_wait(block(o - d, 1 - i, 1 - g, 1 - c))
            attend((o - d) * 2 + 1 - i)

        return carry

    lax.fori_loop(0, o + 1, visit, 0)

    for h in range(heads):
        whole = acc[h]
        att[:, h * VDIM : (h + 1) * VDIM] = (whole[:, :VDIM] / whole[:, VDIM:]).astype(BF16)

    ow_load.wait()
    width = ow.shape[1] // pieces

    def pair_copy(phase, j):
        return pltpu.make_async_remote_copy(
            src_ref=pair_out.at[phase, j],
            dst_ref=pair_in.at[phase, j],
            send_sem=pair_send.at[phase * pieces + j],
            recv_sem=pair_recv.at[phase * pieces + j],
            device_id=mate,
            device_id_type=MESH,
        )

    def cross_copy(j):
        return pltpu.make_async_remote_copy(
            src_ref=cross_out.at[j],
            dst_ref=cross_in.at[j],
            send_sem=cross_send.at[j],
            recv_sem=cross_recv.at[j],
            device_id=across,
            device_id_type=MESH,
        )

    def project(phase, group, j):
        top = att[block_rows(group * 2 + 1 - c), :]
        low_part = att[block_rows(group * 2 + c), :]
        part = dot(jnp.concatenate([top, low_part], axis=0), ow[:, j * width : (j + 1) * width])
        pair_out[phase, j] = part[:rows].astype(BF16)
        kept[phase, j] = part[rows:]
        pair_copy(phase, j).start()

    def cross(j):
        pair_copy(0, j).wait_recv()
        cross_out[j] = (kept[0, j] + pair_in[0, j].astype(F32)).astype(BF16)
        cross_copy(j).start()

    for j in range(pieces):
        project(0, 1 - g, j)
        if j >= 3:
            cross(j - 3)
    for j in range(pieces - 3, pieces):
        cross(j)
    for j in range(pieces):
        project(1, g, j)
    for j in range(pieces):
        pair_copy(1, j).wait_recv()
        cross_copy(j).wait_recv()
        total = kept[1, j] + pair_in[1, j].astype(F32) + cross_in[j].astype(F32)
        out_ref[:, j * width : (j + 1) * width] = total.astype(BF16)

    for d in range(1, O):

        @pl.when(o + d < O)
        def _(d=d):
            up_copy(d).wait_send()

    def drain(d, carry):
        relay_near(d, sent)
        relay_far(d, sent)

        @pl.when((i == 1) | (d > 0))
        def _():
            relay_beside(d, sent)

        return carry

    lax.fori_loop(0, o + 1, drain, 0)
    for copy in q_copies:
        copy.wait_send()
    for j in range(pieces):
        pair_copy(0, j).wait_send()
        pair_copy(1, j).wait_send()
        cross_copy(j).wait_send()


def solution(mesh):
    S, T = mesh.shape["sp"], mesh.shape["tp"]
    assert S % 2 == 0 and T == 4

    def local(tokens, dq, dl, dr, qg, lg, uq, ur, uk, uv, ow):
        rows, depth = tokens.shape
        span = rows * T
        heads = uk.shape[1] // NOPE
        width = ow.shape[1]
        rank = dl.shape[1]
        half = ROPE // 2
        chunks, pieces = 4, 8
        inverse = rope_base ** (-jnp.arange(0, ROPE, 2, dtype=F32) / ROPE)
        positions = lax.axis_index("sp") * span + jnp.arange(span, dtype=jnp.int32)
        angles = positions.astype(F32)[:, None] * jnp.tile(inverse, LANES // half)
        sign = jnp.where(jnp.arange(LANES) % ROPE < half, -1.0, 1.0).astype(F32)
        cosine = jnp.cos(angles)
        sine = jnp.sin(angles) * sign
        O = S // 2
        hbm = pl.BlockSpec(memory_space=pl.ANY)
        vmem = pl.BlockSpec(memory_space=pltpu.VMEM)
        dma = lambda n: pltpu.SemaphoreType.DMA((n,))
        like = lambda a: pltpu.VMEM(a.shape, a.dtype)
        return pl.pallas_call(
            functools.partial(kernel, S, T, chunks, pieces),
            out_shape=jax.ShapeDtypeStruct((rows, width), BF16),
            in_specs=[hbm, hbm, hbm, hbm, vmem, vmem, hbm, hbm, hbm, hbm, hbm, vmem, vmem],
            out_specs=vmem,
            scratch_shapes=[
                like(tokens),
                like(dq),
                like(dl),
                like(dr),
                like(uq),
                like(ur),
                like(uk),
                like(uv),
                like(ow),
                pltpu.VMEM((S * span, rank + LANES), BF16),
                pltpu.VMEM((span, dq.shape[1]), BF16),
                pltpu.VMEM((heads, span, NOPE + LANES), BF16),
                pltpu.VMEM((heads, span, 2 * VDIM), F32),
                pltpu.VMEM((heads, span, LANES), F32),
                pltpu.VMEM((span, heads * VDIM), BF16),
                pltpu.VMEM((2, pieces, rows, width // pieces), BF16),
                pltpu.VMEM((2, pieces, rows, width // pieces), BF16),
                pltpu.VMEM((2, pieces, rows, width // pieces), F32),
                pltpu.VMEM((pieces, rows, width // pieces), BF16),
                pltpu.VMEM((pieces, rows, width // pieces), BF16),
                dma(2 * chunks + 7),
                dma(8 * O),
                dma(S * T),
                dma(3),
                dma(T),
                dma(2 * pieces),
                dma(2 * pieces),
                dma(pieces),
                dma(pieces),
            ],
            compiler_params=pltpu.CompilerParams(
                collective_id=0, has_side_effects=True, vmem_limit_bytes=60 * 1024 * 1024
            ),
        )(
            tokens, dq, dl, dr, qg.reshape(1, -1), lg.reshape(1, -1),
            uq, ur, uk, uv, ow, cosine, sine,
        )

    return jax.shard_map(
        local,
        mesh=mesh,
        in_specs=(
            P(("sp", "tp"), None),
            P(),
            P(),
            P(),
            P(),
            P(),
            P(None, "tp"),
            P(None, "tp"),
            P(None, "tp"),
            P(None, "tp"),
            P("tp", None),
        ),
        out_specs=P(("sp", "tp"), None),
        check_vma=False,
    )
```

time: 125 us -> 67.2 us (0.54); the launches traced: 123 us -> 66.9 us
  Pallas kernels: 0 us -> 61.3 us
  blocking collectives: 51.5 us -> 0 us
  waiting for transfers between devices: 31.6 us -> 0 us
  matrix products: 23.4 us -> 0 us
  between operations: 13.6 us -> 0.02 us
  local copies, waits for them, and re-layouts: 0.13 us -> 4.33 us
    pallas_call x0 -> x1, Pallas kernels: none -> 61.3 us  [local(): pl.pallas_call(functools.partial(kernel, S, T, chunks, pieces), out_shape...]
    all_gather x4 -> x0, blocking collectives: 51.5 us -> none  [the longest x1 32.7 us: local(): lax.all_gather(rotary_rows, 'sp', axis=0, tiled=True)]
    reduce_scatter x1 -> x0, waiting for transfers between devices: 31.6 us -> none  [local(): lax.psum_scatter(jnp.dot(attended, out_weight, preferred_element_type=jnp...]
    dot_general x11 -> x0, matrix products: 23.4 us -> none  [the longest x1 5.12 us: local(): jnp.dot(tokens, down_query, preferred_element_type=jnp.float32)]
    unnamed x16 -> x2, local copies, waits for them, and re-layouts: 0.04 us -> 4.24 us
    reduce_sum x1 -> x0, other arithmetic: 1.5 us -> none  [update(): total = jnp.sum(weights, axis=-1)]
  transfers between devices with their start and end apart: 2 -> 0, of which waited for: 1 -> 0; matrix products, arithmetic and copies ran while one was open for 6% -> 0% of each run, Pallas kernels for 0% -> 0%
where the time goes in v1:
time: 67.2 us; the launch traced here: 66.9 us
  Pallas kernels  61.3 us (91%)
  local copies, waits for them, and re-layouts  4.33 us (6%)
  other arithmetic  1.26 us (2%)
    pallas_call x1, Pallas kernels, local(): pl.pallas_call(functools.partial(kernel, S, T, chunks, pieces), out_shape...  61.3 us
    unnamed x2, local copies, waits for them, and re-layouts  4.24 us

profile of v1, /device:TPU:28, one launch (start us, length us, event | category | flops | bytes accessed | tf_op | source)
XLA Modules:
  0.0 66.9 jit_solution(6086656715281103620)
XLA Ops:
  0.0 0.1 mul.40
  0.1 1.2 %fusion = (f32[256,128]{1,0:T(8,128)}, f32[256,128]{1,0:T(8,128)}) fusion(f32[128]{0:T(128)S(1)} %compare_select_fusion, f32[128]{0:T(128)S(1)} %mul.40, f32[256]{0:T(256)S(1)} %add_convert_fusion), kind=kLoop, calls=%fused_computation.2 | loop fusion | flops 65536 | bytes 264192 | tf_op jit(solution)/shard_map/mul | solution.py:398
  1.4 2.4 %copy.12.dr_hbm = bf16[4096,64]{1,0:T(8,128)(2,1)} copy(bf16[4096,64]{0,1:T(8,128)(2,1)} %param.14) | data formatting | bytes 1048576 | tf_op args[3]
  3.7 61.3 %shard_map.109 = bf16[64,4096]{1,0:T(8,128)(2,1)} custom-call(bf16[64,4096]{1,0:T(8,128)(2,1)} %tokens_hbm.1, bf16[4096,1024]{1,0:T(8,128)(2,1)} %dq_hbm.1, bf16[4096,512]{1,0:T(8,128)(2,1)} %dl_hbm.1, bf16[4096,64]{1,0:T(8,128)(2,1)} %copy.12.dr_hbm, f32[1,1024]{1,0:T(1,128)} %bitcast.2, f32[1,512]{1,0:T(1,128)} %bitcast.3, bf16[1024,512]{1,0:T(8,128)(2,1)} %uq_hbm.1, ...), custom_call_target="tpu_custom_call" | custom-call | tf_op jit(solution)/shard_map/pallas_call | solution.py:404
  65.1 1.9 %copy.14 = bf16[64,4096]{1,0:T(8,128)(2,1)} copy(bf16[64,4096]{1,0:T(8,128)(2,1)} %shard_map.109) | data formatting | bytes 1048576
  (4 shorter events, 0.0 us)

commit v2 on v1

--- a/solution.py
+++ b/solution.py
@@ -2,6 +2,7 @@
 
 import jax
 import jax.numpy as jnp
+import numpy as np
 from jax import lax
 from jax.experimental import pallas as pl
 from jax.experimental.pallas import tpu as pltpu
@@ -24,6 +25,10 @@
 
 def dot(a, b):
     return jnp.dot(a, b, preferred_element_type=F32)
+
+
+def dot_nt(a, b):
+    return lax.dot_general(a, b, (((1,), (1,)), ((), ())), preferred_element_type=F32)
 
 
 def turn(v, cosine, sine):
@@ -52,8 +57,10 @@
     uk_hbm,
     uv_hbm,
     ow_hbm,
-    cos_ref,
-    sin_ref,
+    base_cos,
+    base_sin,
+    row_cos,
+    row_sin,
     out_ref,
     tokens,
     dq,
@@ -75,6 +82,9 @@
     kept,
     cross_out,
     cross_in,
+    uvt,
+    cos_ref,
+    sin_ref,
     load_sem,
     kv_send,
     kv_recv,
@@ -145,13 +155,18 @@
     def kv_wait(b):
         kv_copy(b, mate, 0).wait_recv()
 
+    start_cos, start_sin = base_cos[pl.ds(sp, 1), :], base_sin[pl.ds(sp, 1), :]
+    sign = jnp.where(lax.broadcasted_iota(jnp.int32, (1, LANES), 1) % ROPE < ROPE // 2, -1.0, 1.0)
+    cos_ref[...] = start_cos * row_cos[...] - start_sin * row_sin[...]
+    sin_ref[...] = (start_sin * row_cos[...] + start_cos * row_sin[...]) * sign
+
     tok_load.wait()
     latent = jnp.zeros((rows, rank), F32)
     for k in range(chunks):
         dl_loads[k].wait()
         latent += dot(tokens[:, k * step : (k + 1) * step], dl[k * step : (k + 1) * step, :])
     dr_load.wait()
-    turned = dot(tokens[...], dr[...])
+    turned = dot_nt(tokens[...], dr[...])
     turned = jnp.concatenate([turned, jnp.zeros((rows, LANES - ROPE), F32)], axis=1)
     own_rows = pl.ds(pl.multiple_of(tp * rows, rows), rows)
     mine = block_rows(block(o, i, g, c))
@@ -192,11 +207,20 @@
     def sent(copy):
         copy.wait_send()
 
-    def relay(d):
+    def near(d):
         kv_wait(block(o - d, i, g, c))
         relay_near(d, start)
+
+    def far(d):
         kv_wait(block(o - d, i, 1 - g, c))
         relay_far(d, start)
+
+    def each(first, body):
+        def run(d, carry):
+            body(d)
+            return carry
+
+        lax.fori_loop(first, o + 1, run, 0)
 
     for d in range(1, O):
 
@@ -210,9 +234,6 @@
     for k in range(chunks):
         dq_loads[k].wait()
         query += dot(tokens[:, k * step : (k + 1) * step], dq[k * step : (k + 1) * step, :])
-        if k == chunks // 2 - 1:
-            kv_wait(block(o, i, 1 - g, c))
-            relay_far(0, start)
     ql[own_rows, :] = normed(query, qg_ref[...]).astype(BF16)
 
     def q_copy(t, target, index):
@@ -226,21 +247,22 @@
             device_id_type=MESH,
         )
 
-    far = (1 - g) * 2 + c
-    q_copies = [q_copy(tp, across, 0), q_copy(tp, mate, 1), q_copy(far, mate, 2)]
+    other = (1 - g) * 2 + c
+    q_copies = [q_copy(tp, across, 0), q_copy(tp, mate, 1), q_copy(other, mate, 2)]
     q_copies[0].start()
     q_copies[1].start()
 
-    @pl.when(o >= 1)
-    def _():
-        relay(1)
-
-    q_copy(far, mate, 2).wait_recv()
+    far(0)
+    each(1, near)
+    up_loads[3].wait()
+    uvt[...] = uv[...].T
+
+    q_copy(other, mate, 2).wait_recv()
     q_copies[2].start()
     q_copy(g * 2 + 1 - c, mate, 0).wait_recv()
     q_copy((1 - g) * 2 + 1 - c, mate, 0).wait_recv()
 
-    for copy in up_loads:
+    for copy in up_loads[:3]:
         copy.wait()
     plain = dot(ql[...], uq[...]).astype(BF16)
     turning = dot(ql[...], ur[...])
@@ -251,57 +273,66 @@
         qh[2 * pair + 1, :, NOPE:] = jnp.where(low, pltpu.roll(both, ROPE, 1), 0.0).astype(BF16)
     for h in range(heads):
         qh[h, :, :NOPE] = plain[:, h * NOPE : (h + 1) * NOPE]
-        best[h] = jnp.full((span, LANES), masked_score, F32)
-        acc[h] = jnp.zeros((span, 2 * VDIM), F32)
+        best[h] = jnp.full(best.shape[1:], masked_score, F32)
+        acc[h] = jnp.zeros(acc.shape[1:], F32)
 
     scale = (NOPE + ROPE) ** (-0.5) * log2e
 
-    def attend(s):
+    def attend(s, masked=False):
         part = pl.ds(pl.multiple_of(s * span, span), span)
         lat = kv[part, :rank]
         rot = kv[part, rank:]
         keys = dot(lat, uk[...]).astype(BF16)
-        values = dot(lat, uv[...]).astype(BF16)
-        ones = jnp.ones((span, VDIM), BF16)
-        q_pos = sp * span + lax.broadcasted_iota(jnp.int32, (span, span), 0)
-        k_pos = s * span + lax.broadcasted_iota(jnp.int32, (span, span), 1)
-        allowed = k_pos <= q_pos
+        values = dot_nt(uvt[...], lat).astype(BF16)
+        ones = jnp.ones((acc.shape[1] - VDIM, span), BF16)
+        if masked:
+            k_pos = lax.broadcasted_iota(jnp.int32, (span, span), 0)
+            q_pos = lax.broadcasted_iota(jnp.int32, (span, span), 1)
+            allowed = k_pos <= q_pos
         for h in range(heads):
             key = jnp.concatenate([keys[:, h * NOPE : (h + 1) * NOPE], rot], axis=1)
-            value = jnp.concatenate([values[:, h * VDIM : (h + 1) * VDIM], ones], axis=1)
-            scores = lax.dot_general(qh[h], key, (((1,), (1,)), ((), ())), preferred_element_type=F32)
-            scores = jnp.where(allowed, scores * scale, masked_score)
-            old = best[h][:, :1]
-            new = jnp.maximum(old, jnp.max(scores, axis=-1, keepdims=True))
+            value = jnp.concatenate([values[h * VDIM : (h + 1) * VDIM], ones], axis=0)
+            scores = dot_nt(key, qh[h]) * scale
+            if masked:
+                scores = jnp.where(allowed, scores, masked_score)
+            old = best[h][:1]
+            new = jnp.maximum(old, jnp.max(scores, axis=0, keepdims=True))
             weights = jnp.exp2(scores - new).astype(BF16)
-            acc[h] = acc[h] * jnp.exp2(old - new) + dot(weights, value)
-            best[h] = jnp.broadcast_to(new, (span, LANES))
-
-    def visit(d, carry):
-        @pl.when(d + 2 <= o)
-        def _():
-            relay(d + 2)
-
+            acc[h] = acc[h] * jnp.exp2(old - new) + dot(value, weights)
+            best[h] = jnp.broadcast_to(new, best.shape[1:])
+
+    def own(d, masked=False):
         kv_wait(block(o - d, i, g, 1 - c))
         kv_wait(block(o - d, i, 1 - g, 1 - c))
-        attend((o - d) * 2 + i)
-
-        @pl.when((i == 1) | (d > 0))
+        attend((o - d) * 2 + i, masked)
+
+    def next_to(d):
+        kv_wait(block(o - d, 1 - i, g, c))
+        kv_wait(block(o - d, 1 - i, 1 - g, c))
+        relay_beside(d, start)
+        kv_wait(block(o - d, 1 - i, g, 1 - c))
+        kv_wait(block(o - d, 1 - i, 1 - g, 1 - c))
+        attend((o - d) * 2 + 1 - i)
+
+    def column(d):
+        @pl.when(d < o)
         def _():
-            kv_wait(block(o - d, 1 - i, g, c))
-            kv_wait(block(o - d, 1 - i, 1 - g, c))
-            relay_beside(d, start)
-            kv_wait(block(o - d, 1 - i, g, 1 - c))
-            kv_wait(block(o - d, 1 - i, 1 - g, 1 - c))
-            attend((o - d) * 2 + 1 - i)
-
-        return carry
-
-    lax.fori_loop(0, o + 1, visit, 0)
+            far(d + 1)
+
+        own(d)
+
+    @pl.when(o >= 1)
+    def _():
+        far(1)
+
+    own(0, masked=True)
+    pl.when(i == 1)(lambda: next_to(0))
+    each(1, column)
+    each(1, next_to)
 
     for h in range(heads):
         whole = acc[h]
-        att[:, h * VDIM : (h + 1) * VDIM] = (whole[:, :VDIM] / whole[:, VDIM:]).astype(BF16)
+        att[:, h * VDIM : (h + 1) * VDIM] = (whole[:VDIM] / whole[VDIM : VDIM + 1]).T.astype(BF16)
 
     ow_load.wait()
     width = ow.shape[1] // pieces
@@ -351,7 +382,7 @@
         pair_copy(1, j).wait_recv()
         cross_copy(j).wait_recv()
         total = kept[1, j] + pair_in[1, j].astype(F32) + cross_in[j].astype(F32)
-        out_ref[:, j * width : (j + 1) * width] = total.astype(BF16)
+        out_ref[:, j * width : (j + 1) * width] = total
 
     for d in range(1, O):
 
@@ -388,29 +419,27 @@
         heads = uk.shape[1] // NOPE
         width = ow.shape[1]
         rank = dl.shape[1]
-        half = ROPE // 2
         chunks, pieces = 4, 8
-        inverse = rope_base ** (-jnp.arange(0, ROPE, 2, dtype=F32) / ROPE)
-        positions = lax.axis_index("sp") * span + jnp.arange(span, dtype=jnp.int32)
-        angles = positions.astype(F32)[:, None] * jnp.tile(inverse, LANES // half)
-        sign = jnp.where(jnp.arange(LANES) % ROPE < half, -1.0, 1.0).astype(F32)
-        cosine = jnp.cos(angles)
-        sine = jnp.sin(angles) * sign
+        inverse = np.float32(rope_base) ** (-np.arange(0, ROPE, 2, dtype=np.float32) / np.float32(ROPE))
+        inverse = np.tile(inverse.astype(np.float64), LANES // (ROPE // 2))
+        starts = np.arange(S)[:, None] * span * inverse
+        steps = np.arange(span)[:, None] * inverse
+        tables = [jnp.asarray(f(a), F32) for a in (starts, steps) for f in (np.cos, np.sin)]
         O = S // 2
         hbm = pl.BlockSpec(memory_space=pl.ANY)
         vmem = pl.BlockSpec(memory_space=pltpu.VMEM)
         dma = lambda n: pltpu.SemaphoreType.DMA((n,))
         like = lambda a: pltpu.VMEM(a.shape, a.dtype)
-        return pl.pallas_call(
+        total = pl.pallas_call(
             functools.partial(kernel, S, T, chunks, pieces),
-            out_shape=jax.ShapeDtypeStruct((rows, width), BF16),
-            in_specs=[hbm, hbm, hbm, hbm, vmem, vmem, hbm, hbm, hbm, hbm, hbm, vmem, vmem],
+            out_shape=jax.ShapeDtypeStruct((rows, width), F32),
+            in_specs=[hbm, hbm, hbm, hbm, vmem, vmem, hbm, hbm, hbm, hbm, hbm, vmem, vmem, vmem, vmem],
             out_specs=vmem,
             scratch_shapes=[
                 like(tokens),
                 like(dq),
                 like(dl),
-                like(dr),
+                pltpu.VMEM(dr.shape[::-1], dr.dtype),
                 like(uq),
                 like(ur),
                 like(uk),
@@ -419,14 +448,17 @@
                 pltpu.VMEM((S * span, rank + LANES), BF16),
                 pltpu.VMEM((span, dq.shape[1]), BF16),
                 pltpu.VMEM((heads, span, NOPE + LANES), BF16),
-                pltpu.VMEM((heads, span, 2 * VDIM), F32),
-                pltpu.VMEM((heads, span, LANES), F32),
+                pltpu.VMEM((heads, VDIM + 16, span), F32),
+                pltpu.VMEM((heads, 8, span), F32),
                 pltpu.VMEM((span, heads * VDIM), BF16),
                 pltpu.VMEM((2, pieces, rows, width // pieces), BF16),
                 pltpu.VMEM((2, pieces, rows, width // pieces), BF16),
                 pltpu.VMEM((2, pieces, rows, width // pieces), F32),
                 pltpu.VMEM((pieces, rows, width // pieces), BF16),
                 pltpu.VMEM((pieces, rows, width // pieces), BF16),
+                pltpu.VMEM(uv.shape[::-1], BF16),
+                pltpu.VMEM((span, LANES), F32),
+                pltpu.VMEM((span, LANES), F32),
                 dma(2 * chunks + 7),
                 dma(8 * O),
                 dma(S * T),
@@ -441,9 +473,10 @@
                 collective_id=0, has_side_effects=True, vmem_limit_bytes=60 * 1024 * 1024
             ),
         )(
-            tokens, dq, dl, dr, qg.reshape(1, -1), lg.reshape(1, -1),
-            uq, ur, uk, uv, ow, cosine, sine,
+            tokens, dq, dl, dr.T, qg.reshape(1, -1), lg.reshape(1, -1),
+            uq, ur, uk, uv, ow, *tables,
         )
+        return total.astype(BF16)
 
     return jax.shard_map(
         local,

time: 67.2 us -> 49.4 us (0.74)
  Pallas kernels: 61.3 us -> 47.2 us
  local copies, waits for them, and re-layouts: 4.33 us -> 0 us
  other arithmetic: 1.26 us -> 2.07 us
    pallas_call x1, Pallas kernels: 61.3 us -> 47.2 us  [local(): pl.pallas_call(functools.partial(kernel, S, T, chunks, pieces), out_shape...]
    unnamed x2 -> x0, local copies, waits for them, and re-layouts: 4.24 us -> none
    convert_element_type x1, other arithmetic: 0.01 us -> 2.07 us  [local(): return total.astype(BF16)]
    mul x1 -> x0, other arithmetic: 1.24 us -> none  [local(): sine = jnp.sin(angles) * sign]
where the time goes in v2:
time: 49.4 us; the launch traced here: 49.3 us
  Pallas kernels  47.2 us (96%)
  other arithmetic  2.07 us (4%)
    pallas_call x1, Pallas kernels, local(): pl.pallas_call(functools.partial(kernel, S, T, chunks, pieces), out_shape...  47.2 us
    convert_element_type x1, other arithmetic, local(): return total.astype(BF16)  2.07 us

profile of v2, /device:TPU:28, one launch (start us, length us, event | category | flops | bytes accessed | tf_op | source)
XLA Modules:
  0.0 49.3 jit_solution(7261188857353932559)
XLA Ops:
  0.0 47.2 %shard_map.145 = f32[64,4096]{1,0:T(8,128)} custom-call(bf16[64,4096]{1,0:T(8,128)(2,1)} %tokens_hbm.1, bf16[4096,1024]{1,0:T(8,128)(2,1)} %dq_hbm.1, bf16[4096,512]{1,0:T(8,128)(2,1)} %dl_hbm.1, bf16[64,4096]{1,0:T(8,128)(2,1)} %bitcast.3, f32[1,1024]{1,0:T(1,128)} %bitcast.4, f32[1,512]{1,0:T(1,128)} %bitcast.5, bf16[1024,512]{1,0:T(8,128)(2,1)} %uq_hbm.1, ...), custom_call_target="tpu_custom_call" | custom-call | tf_op jit(solution)/shard_map/pallas_call | solution.py:433
  47.2 2.1 %convert_element_type.3 = bf16[64,4096]{1,0:T(8,128)(2,1)} convert(f32[64,4096]{1,0:T(8,128)} %shard_map.145) | non-fusion elementwise | flops 262144 | bytes 1572864 | tf_op jit(solution)/shard_map/convert_element_type | solution.py:479

commit v3 on v2

--- a/solution.py
+++ b/solution.py
@@ -191,14 +191,22 @@
     def relay_far(d, act):
         b = block(o - d, i, 1 - g, c)
 
-        @pl.when((i == 0) | (d > 0))
+        @pl.when(((i == 0) | (d > 0)) & (d < O - 1))
         def _():
             act(kv_copy(b, beside, 2 * O + 2 * d + 1))
 
         act(kv_copy(b, mate, 4 * O + 4 * d + 1))
 
     def relay_beside(d, act):
-        act(kv_copy(block(o - d, 1 - i, g, c), mate, 4 * O + 4 * d + 2))
+        b = block(o - d, 1 - i, g, c)
+
+        @pl.when(d == O - 1)
+        def _():
+            act(kv_copy(b, across, 2 * O + 2 * d + 1))
+
+        act(kv_copy(b, mate, 4 * O + 4 * d + 2))
+
+    def relay_corner(d, act):
         act(kv_copy(block(o - d, 1 - i, 1 - g, c), mate, 4 * O + 4 * d + 3))
 
     def start(copy):
@@ -262,6 +270,7 @@
     q_copy(g * 2 + 1 - c, mate, 0).wait_recv()
     q_copy((1 - g) * 2 + 1 - c, mate, 0).wait_recv()
 
+    pl.when(o >= 1)(lambda: far(1))
     for copy in up_loads[:3]:
         copy.wait()
     plain = dot(ql[...], uq[...]).astype(BF16)
@@ -306,27 +315,31 @@
         kv_wait(block(o - d, i, 1 - g, 1 - c))
         attend((o - d) * 2 + i, masked)
 
+    def beside_in(d):
+        kv_wait(block(o - d, 1 - i, g, c))
+        relay_beside(d, start)
+
     def next_to(d):
-        kv_wait(block(o - d, 1 - i, g, c))
         kv_wait(block(o - d, 1 - i, 1 - g, c))
-        relay_beside(d, start)
+        relay_corner(d, start)
         kv_wait(block(o - d, 1 - i, g, 1 - c))
         kv_wait(block(o - d, 1 - i, 1 - g, 1 - c))
         attend((o - d) * 2 + 1 - i)
 
     def column(d):
-        @pl.when(d < o)
-        def _():
-            far(d + 1)
-
+        pl.when(d + 3 <= o)(lambda: far(d + 3))
         own(d)
 
-    @pl.when(o >= 1)
+    pl.when(o >= 2)(lambda: far(2))
+    own(0, masked=True)
+    pl.when(o >= 3)(lambda: far(3))
+
+    @pl.when(i == 1)
     def _():
-        far(1)
-
-    own(0, masked=True)
-    pl.when(i == 1)(lambda: next_to(0))
+        beside_in(0)
+        next_to(0)
+
+    each(1, beside_in)
     each(1, column)
     each(1, next_to)
 
@@ -336,6 +349,7 @@
 
     ow_load.wait()
     width = ow.shape[1] // pieces
+    lag = min(5, pieces)
 
     def pair_copy(phase, j):
         return pltpu.make_async_remote_copy(
@@ -372,9 +386,9 @@
 
     for j in range(pieces):
         project(0, 1 - g, j)
-        if j >= 3:
-            cross(j - 3)
-    for j in range(pieces - 3, pieces):
+        if j >= lag:
+            cross(j - lag)
+    for j in range(pieces - lag, pieces):
         cross(j)
     for j in range(pieces):
         project(1, g, j)
@@ -397,6 +411,7 @@
         @pl.when((i == 1) | (d > 0))
         def _():
             relay_beside(d, sent)
+            relay_corner(d, sent)
 
         return carry
 
@@ -419,7 +434,7 @@
         heads = uk.shape[1] // NOPE
         width = ow.shape[1]
         rank = dl.shape[1]
-        chunks, pieces = 4, 8
+        chunks, pieces = 4, 16
         inverse = np.float32(rope_base) ** (-np.arange(0, ROPE, 2, dtype=np.float32) / np.float32(ROPE))
         inverse = np.tile(inverse.astype(np.float64), LANES // (ROPE // 2))
         starts = np.arange(S)[:, None] * span * inverse

time: 49.4 us -> 50.7 us (1.026)
  Pallas kernels: 47.2 us -> 48.5 us
    pallas_call x1, Pallas kernels: 47.2 us -> 48.5 us  [local(): pl.pallas_call(functools.partial(kernel, S, T, chunks, pieces), out_shape...]
where the time goes in v3:
time: 50.7 us; the launch traced here: 50.5 us
  Pallas kernels  48.5 us (96%)
  other arithmetic  2.07 us (4%)
    pallas_call x1, Pallas kernels, local(): pl.pallas_call(functools.partial(kernel, S, T, chunks, pieces), out_shape...  48.5 us
    convert_element_type x1, other arithmetic, local(): return total.astype(BF16)  2.07 us

profile of v3, /device:TPU:28, one launch (start us, length us, event | category | flops | bytes accessed | tf_op | source)
XLA Modules:
  0.0 50.5 jit_solution(7949562200833818785)
XLA Ops:
  0.0 48.5 %shard_map.145 = f32[64,4096]{1,0:T(8,128)} custom-call(bf16[64,4096]{1,0:T(8,128)(2,1)} %tokens_hbm.1, bf16[4096,1024]{1,0:T(8,128)(2,1)} %dq_hbm.1, bf16[4096,512]{1,0:T(8,128)(2,1)} %dl_hbm.1, bf16[64,4096]{1,0:T(8,128)(2,1)} %bitcast.3, f32[1,1024]{1,0:T(1,128)} %bitcast.4, f32[1,512]{1,0:T(1,128)} %bitcast.5, bf16[1024,512]{1,0:T(8,128)(2,1)} %uq_hbm.1, ...), custom_call_target="tpu_custom_call" | custom-call | tf_op jit(solution)/shard_map/pallas_call | solution.py:448
  48.5 2.1 %convert_element_type.3 = bf16[64,4096]{1,0:T(8,128)(2,1)} convert(f32[64,4096]{1,0:T(8,128)} %shard_map.145) | non-fusion elementwise | flops 262144 | bytes 1572864 | tf_op jit(solution)/shard_map/convert_element_type | solution.py:494

commit v4 on v3

--- a/solution.py
+++ b/solution.py
@@ -83,6 +83,8 @@
     cross_out,
     cross_in,
     uvt,
+    first_keys,
+    first_values,
     cos_ref,
     sin_ref,
     load_sem,
@@ -223,6 +225,14 @@
         kv_wait(block(o - d, i, 1 - g, c))
         relay_far(d, start)
 
+    def beside_in(d):
+        kv_wait(block(o - d, 1 - i, g, c))
+        relay_beside(d, start)
+
+    def corner_in(d):
+        kv_wait(block(o - d, 1 - i, 1 - g, c))
+        relay_corner(d, start)
+
     def each(first, body):
         def run(d, carry):
             body(d)
@@ -260,21 +270,38 @@
     q_copies[0].start()
     q_copies[1].start()
 
-    far(0)
-    each(1, near)
+    def kv_heads(s):
+        part = pl.ds(pl.multiple_of(s * span, span), span)
+        lat = kv[part, :rank]
+        return dot(lat, uk[...]).astype(BF16), dot_nt(uvt[...], lat).astype(BF16)
+
+    up_loads[2].wait()
     up_loads[3].wait()
     uvt[...] = uv[...].T
+    far(0)
+    pl.when(o >= 1)(lambda: near(1))
+    kv_wait(block(o, i, g, 1 - c))
+    kv_wait(block(o, i, 1 - g, 1 - c))
+    first_keys[...], first_values[...] = kv_heads(sp)
+    each(2, near)
 
     q_copy(other, mate, 2).wait_recv()
     q_copies[2].start()
+
+    @pl.when(i == 1)
+    def _():
+        beside_in(0)
+        corner_in(0)
+
     q_copy(g * 2 + 1 - c, mate, 0).wait_recv()
     q_copy((1 - g) * 2 + 1 - c, mate, 0).wait_recv()
 
     pl.when(o >= 1)(lambda: far(1))
-    for copy in up_loads[:3]:
+    for copy in up_loads[:2]:
         copy.wait()
-    plain = dot(ql[...], uq[...]).astype(BF16)
-    turning = dot(ql[...], ur[...])
+    scale = (NOPE + ROPE) ** (-0.5) * log2e
+    plain = (dot(ql[...], uq[...]) * scale).astype(BF16)
+    turning = dot(ql[...], ur[...]) * scale
     low = lax.broadcasted_iota(jnp.int32, (span, LANES), 1) < ROPE
     for pair in range(heads // 2):
         both = turn(turning[:, pair * LANES : (pair + 1) * LANES], cos_ref[...], sin_ref[...])
@@ -285,23 +312,25 @@
         best[h] = jnp.full(best.shape[1:], masked_score, F32)
         acc[h] = jnp.zeros(acc.shape[1:], F32)
 
-    scale = (NOPE + ROPE) ** (-0.5) * log2e
-
     def attend(s, masked=False):
-        part = pl.ds(pl.multiple_of(s * span, span), span)
-        lat = kv[part, :rank]
-        rot = kv[part, rank:]
-        keys = dot(lat, uk[...]).astype(BF16)
-        values = dot_nt(uvt[...], lat).astype(BF16)
+        rot = kv[pl.ds(pl.multiple_of(s * span, span), span), rank:]
+        keys, values = (first_keys[...], first_values[...]) if masked else kv_heads(s)
         ones = jnp.ones((acc.shape[1] - VDIM, span), BF16)
         if masked:
             k_pos = lax.broadcasted_iota(jnp.int32, (span, span), 0)
             q_pos = lax.broadcasted_iota(jnp.int32, (span, span), 1)
             allowed = k_pos <= q_pos
+
+        def score(h):
+            key = jnp.concatenate([keys[:, h * NOPE : (h + 1) * NOPE], rot], axis=1)
+            return dot_nt(key, qh[h])
+
+        ahead = score(0)
         for h in range(heads):
-            key = jnp.concatenate([keys[:, h * NOPE : (h + 1) * NOPE], rot], axis=1)
+            scores = ahead
+            if h + 1 < heads:
+                ahead = score(h + 1)
             value = jnp.concatenate([values[h * VDIM : (h + 1) * VDIM], ones], axis=0)
-            scores = dot_nt(key, qh[h]) * scale
             if masked:
                 scores = jnp.where(allowed, scores, masked_score)
             old = best[h][:1]
@@ -310,36 +339,23 @@
             acc[h] = acc[h] * jnp.exp2(old - new) + dot(value, weights)
             best[h] = jnp.broadcast_to(new, best.shape[1:])
 
-    def own(d, masked=False):
-        kv_wait(block(o - d, i, g, 1 - c))
-        kv_wait(block(o - d, i, 1 - g, 1 - c))
-        attend((o - d) * 2 + i, masked)
-
-    def beside_in(d):
-        kv_wait(block(o - d, 1 - i, g, c))
-        relay_beside(d, start)
-
     def next_to(d):
-        kv_wait(block(o - d, 1 - i, 1 - g, c))
-        relay_corner(d, start)
         kv_wait(block(o - d, 1 - i, g, 1 - c))
         kv_wait(block(o - d, 1 - i, 1 - g, 1 - c))
         attend((o - d) * 2 + 1 - i)
 
     def column(d):
         pl.when(d + 3 <= o)(lambda: far(d + 3))
-        own(d)
+        kv_wait(block(o - d, i, g, 1 - c))
+        kv_wait(block(o - d, i, 1 - g, 1 - c))
+        attend((o - d) * 2 + i)
+        corner_in(d)
 
     pl.when(o >= 2)(lambda: far(2))
-    own(0, masked=True)
+    attend(sp, masked=True)
     pl.when(o >= 3)(lambda: far(3))
-
-    @pl.when(i == 1)
-    def _():
-        beside_in(0)
-        next_to(0)
-
     each(1, beside_in)
+    pl.when(i == 1)(lambda: next_to(0))
     each(1, column)
     each(1, next_to)
 
@@ -349,7 +365,7 @@
 
     ow_load.wait()
     width = ow.shape[1] // pieces
-    lag = min(5, pieces)
+    lag = min(3, pieces)
 
     def pair_copy(phase, j):
         return pltpu.make_async_remote_copy(
@@ -434,7 +450,7 @@
         heads = uk.shape[1] // NOPE
         width = ow.shape[1]
         rank = dl.shape[1]
-        chunks, pieces = 4, 16
+        chunks, pieces = 4, 8
         inverse = np.float32(rope_base) ** (-np.arange(0, ROPE, 2, dtype=np.float32) / np.float32(ROPE))
         inverse = np.tile(inverse.astype(np.float64), LANES // (ROPE // 2))
         starts = np.arange(S)[:, None] * span * inverse
@@ -472,6 +488,8 @@
                 pltpu.VMEM((pieces, rows, width // pieces), BF16),
                 pltpu.VMEM((pieces, rows, width // pieces), BF16),
                 pltpu.VMEM(uv.shape[::-1], BF16),
+                pltpu.VMEM((span, heads * NOPE), BF16),
+                pltpu.VMEM((heads * VDIM, span), BF16),
                 pltpu.VMEM((span, LANES), F32),
                 pltpu.VMEM((span, LANES), F32),
                 dma(2 * chunks + 7),

time: 50.7 us -> 45.3 us (0.89)
  Pallas kernels: 48.5 us -> 42.6 us
    pallas_call x1, Pallas kernels: 48.5 us -> 42.6 us  [local(): pl.pallas_call(functools.partial(kernel, S, T, chunks, pieces), out_shape...]
where the time goes in v4:
time: 45.3 us; the launch traced here: 44.7 us
  Pallas kernels  42.6 us (94%)
  other arithmetic  2.07 us (5%)
    pallas_call x1, Pallas kernels, local(): pl.pallas_call(functools.partial(kernel, S, T, chunks, pieces), out_shape...  42.6 us
    convert_element_type x1, other arithmetic, local(): return total.astype(BF16)  2.07 us

profile of v4, /device:TPU:28, one launch (start us, length us, event | category | flops | bytes accessed | tf_op | source)
XLA Modules:
  0.0 44.7 jit_solution(6125015840892734539)
XLA Ops:
  0.0 42.6 %shard_map.145 = f32[64,4096]{1,0:T(8,128)} custom-call(bf16[64,4096]{1,0:T(8,128)(2,1)} %tokens_hbm.1, bf16[4096,1024]{1,0:T(8,128)(2,1)} %dq_hbm.1, bf16[4096,512]{1,0:T(8,128)(2,1)} %dl_hbm.1, bf16[64,4096]{1,0:T(8,128)(2,1)} %bitcast.3, f32[1,1024]{1,0:T(1,128)} %bitcast.4, f32[1,512]{1,0:T(1,128)} %bitcast.5, bf16[1024,512]{1,0:T(8,128)(2,1)} %uq_hbm.1, ...), custom_call_target="tpu_custom_call" | custom-call | tf_op jit(solution)/shard_map/pallas_call | solution.py:464
  42.6 2.1 %convert_element_type.3 = bf16[64,4096]{1,0:T(8,128)(2,1)} convert(f32[64,4096]{1,0:T(8,128)} %shard_map.145) | non-fusion elementwise | flops 262144 | bytes 1572864 | tf_op jit(solution)/shard_map/convert_element_type | solution.py:512

commit v5 on v4

--- a/solution.py
+++ b/solution.py
@@ -351,11 +351,11 @@
         attend((o - d) * 2 + i)
         corner_in(d)
 
+    attend(sp, masked=True)
     pl.when(o >= 2)(lambda: far(2))
-    attend(sp, masked=True)
+    pl.when(i == 1)(lambda: next_to(0))
     pl.when(o >= 3)(lambda: far(3))
     each(1, beside_in)
-    pl.when(i == 1)(lambda: next_to(0))
     each(1, column)
     each(1, next_to)
 

time: 45.3 us -> 45.3 us (level)
  the two profiles are of different devices: /device:TPU:28 before, /device:TPU:25 now
where the time goes in v5:
time: 45.3 us; the launch traced here: 45.1 us
  Pallas kernels  43 us (95%)
  other arithmetic  2.07 us (5%)
    pallas_call x1, Pallas kernels, local(): pl.pallas_call(functools.partial(kernel, S, T, chunks, pieces), out_shape...  43 us
    convert_element_type x1, other arithmetic, local(): return total.astype(BF16)  2.07 us

profile of v5, /device:TPU:25, one launch (start us, length us, event | category | flops | bytes accessed | tf_op | source)
XLA Modules:
  0.0 45.1 jit_solution(7947134654214964572)
XLA Ops:
  0.0 43.0 %shard_map.145 = f32[64,4096]{1,0:T(8,128)} custom-call(bf16[64,4096]{1,0:T(8,128)(2,1)} %tokens_hbm.1, bf16[4096,1024]{1,0:T(8,128)(2,1)} %dq_hbm.1, bf16[4096,512]{1,0:T(8,128)(2,1)} %dl_hbm.1, bf16[64,4096]{1,0:T(8,128)(2,1)} %bitcast.3, f32[1,1024]{1,0:T(1,128)} %bitcast.4, f32[1,512]{1,0:T(1,128)} %bitcast.5, bf16[1024,512]{1,0:T(8,128)(2,1)} %uq_hbm.1, ...), custom_call_target="tpu_custom_call" | custom-call | tf_op jit(solution)/shard_map/pallas_call | solution.py:464
  43.1 2.1 %convert_element_type.3 = bf16[64,4096]{1,0:T(8,128)(2,1)} convert(f32[64,4096]{1,0:T(8,128)} %shard_map.145) | non-fusion elementwise | flops 262144 | bytes 1572864 | tf_op jit(solution)/shard_map/convert_element_type | solution.py:512
